TPU v7x, 32 devices: a whole 2x2x4 slice. The times are simulated.
32 devices in a mesh: ep: 32 (over z, y, x, core).
Axes of the slice: x: 2, y: 2, z: 4, core: 2. Of those that a mesh axis runs over, the one named last changes fastest.
Arguments:
- tokens: bfloat16 [128, 2048], P('ep'), may hold values from -6 to 6
- lengths: int32 [128], P('ep'), may hold values from 1 to 1023
- cache_keys: bfloat16 [128, 1024, 2, 128], P('ep')
- cache_values: bfloat16 [128, 1024, 2, 128], P('ep'), may hold values from -6 to 6
- query_w: bfloat16 [2048, 1024], replicated, may hold values from -0.125 to 0.125
- key_w: bfloat16 [2048, 256], replicated, may hold values from -0.125 to 0.125
- value_w: bfloat16 [2048, 256], replicated, may hold values from -0.125 to 0.125
- out_w: bfloat16 [1024, 2048], replicated, may hold values from -0.1875 to 0.1875
- mix_lambda: float32 [8], replicated, may hold values from 0.3 to 0.8
- head_gain: float32 [128], replicated, may hold values from 0.1 to 1.9
- attn_gain: float32 [2048], replicated, may hold values from 0.1 to 1.9
- ffn_gain: float32 [2048], replicated, may hold values from 0.1 to 1.9
- routes: int32 [128, 2], P('ep'), may hold values from 0 to 1, all different within a row; in each aligned block of 4 rows (0 to 3, 4 to 7, ...) at most 4 rows name the same one
- route_weights: float32 [128, 2], P('ep'), may hold values from 0.2 to 1
- exp_gate: bfloat16 [2048, 12288], P(None, 'ep'), may hold values from -0.125 to 0.125
- exp_up: bfloat16 [2048, 12288], P(None, 'ep'), may hold values from -0.125 to 0.125
- exp_down: bfloat16 [12288, 2048], P('ep'), may hold values from -0.078125 to 0.078125
- dense_gate: bfloat16 [32, 1024, 352], P('ep'), may hold values from -0.125 to 0.125
- dense_up: bfloat16 [32, 1024, 352], P('ep'), may hold values from -0.125 to 0.125
- dense_down: bfloat16 [32, 352, 1024], P('ep'), may hold values from -0.078125 to 0.078125
- branch_gate: bfloat16 [2048], replicated, may hold values from -0.125 to 0.125
Outputs:
- output: bfloat16 [128, 2048], P('ep')
- new_keys: bfloat16 [128, 256], P('ep')
- new_values: bfloat16 [128, 256], P('ep')
Inputs may be any that keep to these rules, and one draw needn't show every extreme that they name: `routes`: each row names 2 different experts; among the 4 rows of one device no expert is named by more than 4 rows, a bound that some block reaches.
All inputs are finite; a program needn't handle non-finite values.
Results may differ from a plain program's by a relative error of at most 0.015.
Values may be sent and summed in bfloat16 or wider, within the bound.
A program may use at most 128 MiB of HBM per device.

v0:
```python
import functools

import jax
import jax.numpy as jnp
from jax import lax
from jax.experimental import pallas as pl
from jax.experimental.pallas import tpu as pltpu
from jax.sharding import PartitionSpec as P

HEADS = 8
KV_HEADS = 2
HEAD_DIM = 128
SPLIT = 16
SIDE = 128
QKV_CHUNKS = 4
ROW_CHUNK = 128

F32 = jnp.float32
BF16 = jnp.bfloat16
MESH = pl.DeviceIdType.MESH


def attention_part(
    experts,
    small,
    keys,
    values,
    query_w,
    key_w,
    value_w,
    out_w,
    ext,
    hidden,
    new_keys,
    new_values,
    kbuf,
    vbuf,
    qbuf,
    kwbuf,
    vwbuf,
    obuf,
    qscr,
    hscr,
    wsem,
    ksem,
    vsem,
    osem,
    more_loads,
):
    tokens, lengths, lam, head_gain, attn_gain, ffn_gain, routes, route_weights, branch_gate = [
        dst for _, dst in small[0]
    ]
    rows, width = tokens.shape
    span = keys.shape[1]
    step = width // QKV_CHUNKS
    groups = HEADS // KV_HEADS
    half = HEAD_DIM // 2
    small_copies = [
        pltpu.make_async_copy(src, dst, small[1].at[i]) for i, (src, dst) in enumerate(small[0])
    ]
    for copy in small_copies:
        copy.start()
    weight_copies = []
    for c in range(QKV_CHUNKS):
        part = pl.ds(c * step, step)
        trio = [
            pltpu.make_async_copy(src.at[part], dst.at[part], wsem.at[3 * c + i])
            for i, (src, dst) in enumerate(((query_w, qbuf), (key_w, kwbuf), (value_w, vwbuf)))
        ]
        for copy in trio:
            copy.start()
        weight_copies.append(trio)
    key_copies = [pltpu.make_async_copy(keys.at[s], kbuf.at[s], ksem.at[s]) for s in range(rows)]
    value_copies = [pltpu.make_async_copy(values.at[s], vbuf.at[s], vsem.at[s]) for s in range(rows)]
    for s in range(rows):
        key_copies[s].start()
        value_copies[s].start()
    out_copy = pltpu.make_async_copy(out_w, obuf, osem.at[0])
    out_copy.start()
    for copy in more_loads:
        copy.start()
    for copy in small_copies:
        copy.wait()

    x = tokens[...].astype(F32)
    normed = x * lax.rsqrt(jnp.mean(x * x, axis=-1, keepdims=True) + 1e-06) * attn_gain[...]
    normed = normed.astype(BF16)
    query = jnp.zeros((rows, query_w.shape[1]), F32)
    knew = jnp.zeros((rows, key_w.shape[1]), F32)
    vnew = jnp.zeros((rows, value_w.shape[1]), F32)
    for c in range(QKV_CHUNKS):
        for copy in weight_copies[c]:
            copy.wait()
        part = slice(c * step, (c + 1) * step)
        left = normed[:, part]
        query += jnp.dot(left, qbuf[part, :], preferred_element_type=F32)
        knew += jnp.dot(left, kwbuf[part, :], preferred_element_type=F32)
        vnew += jnp.dot(left, vwbuf[part, :], preferred_element_type=F32)
    new_keys[...] = knew.astype(BF16)
    new_values[...] = vnew.astype(BF16)
    query = query.astype(BF16).astype(F32)
    knew = knew.astype(BF16).astype(F32)
    vnew = vnew.astype(BF16).astype(F32)
    for s in range(rows):
        for h in range(HEADS):
            qscr[s, h : h + 1, :] = query[s : s + 1, h * HEAD_DIM : (h + 1) * HEAD_DIM]

    scale = half ** (-0.5)
    lane = lax.broadcasted_iota(jnp.int32, (HEADS, HEAD_DIM), 1)
    head_row = lax.broadcasted_iota(jnp.int32, (HEADS, HEAD_DIM), 0)
    col = lax.broadcasted_iota(jnp.int32, (2 * HEADS, span), 1)
    row = lax.broadcasted_iota(jnp.int32, (2 * HEADS, span), 0)
    own_group = (col % KV_HEADS) == ((row % HEADS) // groups)
    head_col = lax.broadcasted_iota(jnp.int32, (HEADS, 1), 0)
    lam_col = jnp.zeros((HEADS, 1), F32)
    for h in range(HEADS):
        lam_col = jnp.where(head_col == h, lam[h], lam_col)
    for s in range(rows):
        q = qscr[s]
        both = jnp.concatenate([jnp.where(lane < half, q, 0.0), jnp.where(lane >= half, q, 0.0)], axis=0)
        kown = jnp.zeros((HEADS, HEAD_DIM), F32)
        vown = jnp.zeros((HEADS, HEAD_DIM), F32)
        for g in range(KV_HEADS):
            mine = head_row // groups == g
            part = slice(g * HEAD_DIM, (g + 1) * HEAD_DIM)
            kown = jnp.where(mine, knew[s : s + 1, part], kown)
            vown = jnp.where(mine, vnew[s : s + 1, part], vown)
        own = jnp.sum(both * jnp.concatenate([kown, kown], axis=0), axis=-1, keepdims=True) * scale
        key_copies[s].wait()
        scores = lax.dot_general(
            both.astype(BF16), kbuf[s], (((1,), (1,)), ((), ())), preferred_element_type=F32
        ) * scale
        valid = own_group & (col < KV_HEADS * lengths[s])
        largest = jnp.maximum(
            jnp.max(jnp.where(valid, scores, -jnp.inf), axis=-1, keepdims=True), own
        )
        raised = jnp.where(valid, jnp.exp(scores - largest), 0.0)
        own_raised = jnp.exp(own - largest)
        inverse = 1.0 / (jnp.sum(raised, axis=-1, keepdims=True) + own_raised)
        prob = raised * inverse
        own_prob = own_raised * inverse
        weights = (prob[:HEADS] - lam_col * prob[HEADS:]).astype(BF16)
        own_weights = (own_prob[:HEADS] - lam_col * own_prob[HEADS:]).astype(BF16).astype(F32)
        value_copies[s].wait()
        mixed = jnp.dot(weights, vbuf[s], preferred_element_type=F32) + own_weights * vown
        normal = mixed * lax.rsqrt(jnp.mean(mixed * mixed, axis=-1, keepdims=True) + 1e-05)
        normal = normal * head_gain[...]
        for h in range(HEADS):
            hscr[s : s + 1, h * HEAD_DIM : (h + 1) * HEAD_DIM] = normal[h : h + 1, :]
    out_copy.wait()
    state = x + jnp.dot(hscr[...].astype(BF16), obuf[...], preferred_element_type=F32)
    hidden[...] = state
    ffn = state * lax.rsqrt(jnp.mean(state * state, axis=-1, keepdims=True) + 1e-06)
    ffn = (ffn * ffn_gain[...]).astype(BF16)
    ext[:, :width] = ffn
    pieces = jnp.zeros((rows, SIDE), F32)
    branch = branch_gate[...].astype(F32)
    for c in range(width // SIDE):
        pieces += ffn[:, c * SIDE : (c + 1) * SIDE].astype(F32) * branch[c : c + 1, :]
    logit = jnp.sum(pieces, axis=-1, keepdims=True)
    gate = 1.0 / (1.0 + jnp.exp(-logit))
    spot = lax.broadcasted_iota(jnp.int32, (rows, SIDE), 1)
    name = spot % (SIDE // 2)
    table = jnp.where(name == experts, gate, 0.0)
    token_row = lax.broadcasted_iota(jnp.int32, (rows, SIDE), 0)
    for k in range(routes.shape[0]):
        for s in range(rows):
            here = (name == routes[k, s]) & (name < experts) & (token_row == s)
            table = table + jnp.where(here, route_weights[k, s], 0.0)
    high = table.astype(BF16).astype(F32)
    ext[:, width:] = jnp.where(spot < SIDE // 2, high, table - high).astype(BF16)


def layer_kernel(
    n,
    tokens,
    lengths,
    lam,
    head_gain,
    attn_gain,
    ffn_gain,
    routes,
    route_weights,
    branch_gate,
    keys,
    values,
    query_w,
    key_w,
    value_w,
    out_w,
    exp_gate,
    exp_up,
    exp_down,
    dense_gate,
    dense_up,
    dense_down,
    out,
    new_keys,
    new_values,
    tokens_v,
    lengths_v,
    lam_v,
    head_gain_v,
    attn_gain_v,
    ffn_gain_v,
    routes_v,
    route_weights_v,
    branch_gate_v,
    small_sem,
    ext,
    hidden,
    kbuf,
    vbuf,
    qbuf,
    kwbuf,
    vwbuf,
    obuf,
    qscr,
    hscr,
    asem,
    ksem,
    vsem,
    osem,
    egbuf,
    eubuf,
    edbuf,
    dgbuf,
    dubuf,
    ddbuf,
    recv,
    xall,
    gpart,
    upart,
    gsend,
    usend,
    grecv,
    urecv,
    act,
    total,
    sib_send,
    sib_recv,
    rs_send,
    rs_recv,
    wsem,
    ag_send_sem,
    ag_recv_sem,
    fw_send_sem,
    fw_recv_sem,
    ex_send_sem,
    ex_recv_sem,
    sib_send_sem,
    sib_recv_sem,
    rs_send_sem,
    rs_recv_sem,
):
    me = lax.axis_index("ep")
    chips = n // 2
    chip, core = me // 2, lax.rem(me, 2)
    sibling = chip * 2 + 1 - core
    blocks = n // SPLIT
    experts = n // SPLIT
    rows, width = hidden.shape
    total_rows = n * rows
    chunk = min(ROW_CHUNK, total_rows)
    row_span = dense_gate.shape[2]

    def at(k):
        return lax.rem(chip + k, chips) * 2 + core

    gchips = SPLIT // 2
    block = me // SPLIT
    expert = me // SPLIT
    gchip = lax.rem(me, SPLIT) // 2
    group_rows = SPLIT * rows

    def mate(j):
        return block * SPLIT + lax.rem(gchip + j, gchips) * 2 + core

    def group(d):
        return lax.rem(block + d, blocks)

    def place(d, j):
        return group(d) * gchips + lax.rem(gchip + j, gchips)

    def source(b, j):
        home = lax.rem(block + blocks - b, blocks)
        return home * SPLIT + lax.rem(gchip + gchips - j, gchips) * 2 + core

    loads = [
        pltpu.make_async_copy(src, dst, wsem.at[i])
        for i, (src, dst) in enumerate(
            (
                (dense_gate.at[0], dgbuf),
                (dense_up.at[0], dubuf),
                (exp_gate, egbuf),
                (exp_up, eubuf),
                (exp_down, edbuf),
                (dense_down.at[0], ddbuf),
            )
        )
    ]
    barrier = pltpu.get_barrier_semaphore()

    def greet(k, carry):
        pl.semaphore_signal(barrier, inc=1, device_id=(at(k),), device_id_type=MESH)
        return carry

    lax.fori_loop(1, chips, greet, 0)
    pl.semaphore_signal(barrier, inc=1, device_id=(sibling,), device_id_type=MESH)
    small = [
        (tokens, tokens_v),
        (lengths, lengths_v),
        (lam, lam_v),
        (head_gain, head_gain_v),
        (attn_gain, attn_gain_v),
        (ffn_gain, ffn_gain_v),
        (routes, routes_v),
        (route_weights, route_weights_v),
        (branch_gate, branch_gate_v),
    ]
    attention_part(
        experts, (small, small_sem), keys, values, query_w, key_w, value_w, out_w, ext, hidden,
        new_keys, new_values, kbuf, vbuf, qbuf, kwbuf, vwbuf, obuf, qscr, hscr,
        asem, ksem, vsem, osem, loads,
    )
    pl.semaphore_wait(barrier, chips)

    def send_block(ref, owner, q, target):
        return pltpu.make_async_remote_copy(
            src_ref=ref,
            dst_ref=recv.at[owner],
            send_sem=ag_send_sem.at[q],
            recv_sem=ag_recv_sem.at[q],
            device_id=(target,),
            device_id_type=MESH,
        )

    def near_copy(j):
        return send_block(ext, me, j, mate(j))

    def far_copy(b):
        return send_block(ext, me, b * gchips, group(b) * SPLIT + lax.rem(me, SPLIT))

    def relay_copy(b, j):
        owner = source(b, 0)
        return send_block(recv.at[owner], owner, b * gchips + j, mate(j))

    def fw_copy(b, j):
        owner = source(b, j)
        return pltpu.make_async_remote_copy(
            src_ref=recv.at[owner],
            dst_ref=recv.at[owner],
            send_sem=fw_send_sem.at[b * gchips + j],
            recv_sem=fw_recv_sem.at[b * gchips + j],
            device_id=(sibling,),
            device_id_type=MESH,
        )

    own_copy = pltpu.make_async_remote_copy(
        src_ref=ext,
        dst_ref=recv.at[me],
        send_sem=fw_send_sem.at[0],
        recv_sem=fw_recv_sem.at[0],
        device_id=(sibling,),
        device_id_type=MESH,
    )

    def loop(low, high, body):
        def run(i, carry):
            body(i)
            return carry

        lax.fori_loop(low, high, run, 0)

    for b in range(1, blocks):
        far_copy(b).start()
    loop(1, gchips, lambda j: near_copy(j).start())
    own_copy.start()
    recv[me] = ext[...]
    for b in range(1, blocks):
        far_copy(b).wait_recv()
        loop(1, gchips, lambda j: relay_copy(b, j).start())
        fw_copy(b, 0).start()

    def near_forward(j):
        near_copy(j).wait_recv()
        fw_copy(0, j).start()

    loop(1, gchips, near_forward)
    own_copy.wait_recv()
    loop(1, gchips, lambda j: fw_copy(0, j).wait_recv())

    def widen(home):
        def one(i):
            c = home * gchips + i
            pair = jnp.concatenate([recv[2 * c].astype(F32), recv[2 * c + 1].astype(F32)], axis=0)
            xall[pl.ds(pl.multiple_of(c * 2 * rows, 2 * rows), 2 * rows), :] = pair

        loop(0, gchips, one)

    def group_part(d):
        return pl.ds(pl.multiple_of(group(d) * group_rows, group_rows), group_rows)

    def by_rows(body):
        if total_rows == chunk:
            body(pl.ds(0, chunk))
        else:

            def run(r, carry):
                body(pl.ds(pl.multiple_of(r * chunk, chunk), chunk))
                return carry

            lax.fori_loop(0, total_rows // chunk, run, 0)

    loads[0].wait()
    loads[1].wait()

    def dense_in(part):
        left = xall[part, pl.ds(pl.multiple_of(block * row_span, 128), row_span)].astype(BF16)
        across = (((1,), (1,)), ((), ()))
        g = lax.dot_general(left, dgbuf[...], across, preferred_element_type=F32)
        u = lax.dot_general(left, dubuf[...], across, preferred_element_type=F32)
        gpart[part, :] = g
        upart[part, :] = u
        gsend[part, :] = g.astype(BF16)
        usend[part, :] = u.astype(BF16)

    def exchange(b):
        part = group_part(b)
        copies = []
        for j in range(1, blocks):
            for i, (src, dst) in enumerate(((gsend, grecv), (usend, urecv))):
                slot = 2 * (b * (blocks - 1) + j - 1) + i
                copies.append(
                    pltpu.make_async_remote_copy(
                        src_ref=src.at[part],
                        dst_ref=dst.at[j - 1, part],
                        send_sem=ex_send_sem.at[slot],
                        recv_sem=ex_recv_sem.at[slot],
                        device_id=(lax.rem(me + j * SPLIT, n),),
                        device_id_type=MESH,
                    )
                )
        for copy in copies:
            copy.start()
        return copies

    widen(block)
    dense_in(group_part(0))
    exchanges = [exchange(0)]
    for b in range(1, blocks):

        def relay_forward(j):
            relay_copy(b, j).wait_recv()
            fw_copy(b, j).start()

        loop(1, gchips, relay_forward)
    for b in range(1, blocks):
        loop(0, gchips, lambda j: fw_copy(b, j).wait_recv())
    for b in range(1, blocks):
        widen(group(b))
        dense_in(group_part(b))
        exchanges.append(exchange(b))

    loads[2].wait()
    loads[3].wait()

    def expert_in(part):
        left = xall[part, :width].astype(BF16)
        g = jnp.dot(left, egbuf[...], preferred_element_type=F32)
        u = jnp.dot(left, eubuf[...], preferred_element_type=F32)
        act[part, :] = (g / (1.0 + jnp.exp(-g)) * u).astype(BF16)

    by_rows(expert_in)
    loads[4].wait()

    def side_value(part, which):
        side = xall[part, width:]
        spot = lax.broadcasted_iota(jnp.int32, side.shape, 1) % (SIDE // 2)
        return jnp.sum(jnp.where(spot == which, side, 0.0), axis=-1, keepdims=True)

    def expert_out(part):
        product = jnp.dot(act[part, :], edbuf[...], preferred_element_type=F32)
        total[part, :] = product * side_value(part, expert)

    by_rows(expert_out)
    loads[5].wait()

    def dense_out(part):
        g = gpart[part, :]
        u = upart[part, :]
        for j in range(blocks - 1):
            g = g + grecv[j, part, :].astype(F32)
            u = u + urecv[j, part, :].astype(F32)
        dact = (g / (1.0 + jnp.exp(-g)) * u).astype(BF16)
        product = jnp.dot(dact, ddbuf[...], preferred_element_type=F32)
        cols = pl.ds(pl.multiple_of(block * row_span, 128), row_span)
        total[part, cols] = total[part, cols] + product * side_value(part, experts)

    def both_halves(d, j):
        c = place(d, j)
        pair = total[pl.ds(pl.multiple_of(c * 2 * rows, 2 * rows), 2 * rows), :]
        return pair[:rows], pair[rows:]

    def sib_copy(q):
        return pltpu.make_async_remote_copy(
            src_ref=sib_send.at[q],
            dst_ref=sib_recv.at[q],
            send_sem=sib_send_sem.at[q],
            recv_sem=sib_recv_sem.at[q],
            device_id=(sibling,),
            device_id_type=MESH,
        )

    def rs_copy(d, j):
        q = d * gchips + j
        return pltpu.make_async_remote_copy(
            src_ref=rs_send.at[q],
            dst_ref=rs_recv.at[q],
            send_sem=rs_send_sem.at[q],
            recv_sem=rs_recv_sem.at[q],
            device_id=(place(d, j) * 2 + core,),
            device_id_type=MESH,
        )

    def add_sibling(d, j):
        q = d * gchips + j
        sib_copy(q).wait_recv()
        low, high = both_halves(d, j)
        return jnp.where(core == 0, low, high) + sib_recv[q].astype(F32)

    for d in list(range(1, blocks)) + [0]:
        for j in range(1, blocks):
            first = 2 * (j - 1)
            for copy in exchanges[(j + d) % blocks][first : first + 2]:
                copy.wait_recv()
        dense_out(group_part(d))

        def pack(j):
            low, high = both_halves(d, j)
            sib_send[d * gchips + j] = jnp.where(core == 0, high, low).astype(BF16)

        def forward(j):
            rs_send[d * gchips + j] = add_sibling(d, j).astype(BF16)
            rs_copy(d, j).start()

        loop(0, gchips, pack)
        loop(0, gchips, lambda j: sib_copy(d * gchips + j).start())
        loop(1 if d == 0 else 0, gchips, forward)
    result = hidden[...] + add_sibling(0, 0)

    def collect(q, acc):
        rs_copy(q // gchips, lax.rem(q, gchips)).wait_recv()
        return acc + rs_recv[q].astype(F32)

    result = lax.fori_loop(1, chips, collect, result)
    out[...] = result.astype(BF16)

    for b in range(1, blocks):
        far_copy(b).wait_send()
        loop(1, gchips, lambda j: relay_copy(b, j).wait_send())
        loop(0, gchips, lambda j: fw_copy(b, j).wait_send())
        loop(0, gchips, lambda j: rs_copy(b, j).wait_send())
    own_copy.wait_send()

    def drain(j):
        near_copy(j).wait_send()
        fw_copy(0, j).wait_send()
        rs_copy(0, j).wait_send()

    loop(1, gchips, drain)
    loop(0, chips, lambda q: sib_copy(q).wait_send())
    for copies in exchanges:
        for copy in copies:
            copy.wait_send()


def finish_kernel(count, *refs):
    sources, targets, held = refs[:count], refs[count : 2 * count], refs[2 * count : 3 * count]
    in_sem, out_sem = refs[3 * count :]
    ins = [pltpu.make_async_copy(sources[i], held[i], in_sem.at[i]) for i in range(count)]
    outs = [pltpu.make_async_copy(held[i], targets[i], out_sem.at[i]) for i in range(count)]
    for copy in ins:
        copy.start()
    for i in range(count):
        ins[i].wait()
        outs[i].start()
    for copy in outs:
        copy.wait()


def per_device(
    n,
    tokens,
    lengths,
    cache_keys,
    cache_values,
    query_w,
    key_w,
    value_w,
    out_w,
    mix_lambda,
    head_gain,
    attn_gain,
    ffn_gain,
    routes,
    route_weights,
    exp_gate,
    exp_up,
    exp_down,
    dense_gate,
    dense_up,
    dense_down,
    branch_gate,
):
    rows, width = tokens.shape
    cache_len = cache_keys.shape[1]
    span = cache_len * KV_HEADS
    experts = n // SPLIT
    vmem = pl.BlockSpec(memory_space=pltpu.VMEM)
    anywhere = pl.BlockSpec(memory_space=pl.ANY)
    all_rows = n * rows
    chips = n // 2
    cols = dense_gate.shape[2]
    others = max(1, n // SPLIT - 1)
    sem = pltpu.SemaphoreType.DMA
    dense_gate = jnp.swapaxes(dense_gate, 1, 2)
    dense_up = jnp.swapaxes(dense_up, 1, 2)
    routes = routes.T
    route_weights = route_weights.T
    results = pl.pallas_call(
        functools.partial(layer_kernel, n),
        name="layer",
        out_shape=(
            jax.ShapeDtypeStruct((rows, width), BF16),
            jax.ShapeDtypeStruct((rows, key_w.shape[1]), BF16),
            jax.ShapeDtypeStruct((rows, value_w.shape[1]), BF16),
        ),
        in_specs=[anywhere] * 21,
        out_specs=(vmem,) * 3,
        scratch_shapes=[
            pltpu.VMEM((rows, width), BF16),
            pltpu.SMEM(lengths.shape, jnp.int32),
            pltpu.SMEM(mix_lambda.shape, F32),
            pltpu.VMEM((1, HEAD_DIM), F32),
            pltpu.VMEM((1, width), F32),
            pltpu.VMEM((1, width), F32),
            pltpu.SMEM(routes.shape, jnp.int32),
            pltpu.SMEM(route_weights.shape, F32),
            pltpu.VMEM((width // SIDE, SIDE), BF16),
            sem((9,)),
            pltpu.VMEM((rows, width + SIDE), BF16),
            pltpu.VMEM((rows, width), F32),
            pltpu.VMEM((rows, span, HEAD_DIM), BF16),
            pltpu.VMEM((rows, span, HEAD_DIM), BF16),
            pltpu.VMEM(query_w.shape, BF16),
            pltpu.VMEM(key_w.shape, BF16),
            pltpu.VMEM(value_w.shape, BF16),
            pltpu.VMEM(out_w.shape, BF16),
            pltpu.VMEM((rows, HEADS, HEAD_DIM), F32),
            pltpu.VMEM((rows, HEADS * HEAD_DIM), F32),
            sem((3 * QKV_CHUNKS,)),
            sem((rows,)),
            sem((rows,)),
            sem((1,)),
            pltpu.VMEM(exp_gate.shape, BF16),
            pltpu.VMEM(exp_up.shape, BF16),
            pltpu.VMEM(exp_down.shape, BF16),
            pltpu.VMEM(dense_gate.shape[1:], BF16),
            pltpu.VMEM(dense_up.shape[1:], BF16),
            pltpu.VMEM(dense_down.shape[1:], BF16),
            pltpu.VMEM((n, rows, width + SIDE), BF16),
            pltpu.VMEM((all_rows, width + SIDE), F32),
            pltpu.VMEM((all_rows, cols), F32),
            pltpu.VMEM((all_rows, cols), F32),
            pltpu.VMEM((all_rows, cols), BF16),
            pltpu.VMEM((all_rows, cols), BF16),
            pltpu.VMEM((others, all_rows, cols), BF16),
            pltpu.VMEM((others, all_rows, cols), BF16),
            pltpu.VMEM((all_rows, exp_gate.shape[1]), BF16),
            pltpu.VMEM((all_rows, width), F32),
            pltpu.VMEM((chips, rows, width), BF16),
            pltpu.VMEM((chips, rows, width), BF16),
            pltpu.VMEM((chips, rows, width), BF16),
            pltpu.VMEM((chips, rows, width), BF16),
            sem((6,)),
            sem((chips,)),
            sem((chips,)),
            sem((chips,)),
            sem((chips,)),
            sem((2 * others * (n // SPLIT),)),
            sem((2 * others * (n // SPLIT),)),
            sem((chips,)),
            sem((chips,)),
            sem((chips,)),
            sem((chips,)),
        ],
        compiler_params=pltpu.CompilerParams(
            collective_id=0, has_side_effects=True, vmem_limit_bytes=63 * 2**20
        ),
    )(
        tokens,
        lengths,
        mix_lambda,
        head_gain.reshape(1, HEAD_DIM),
        attn_gain.reshape(1, width),
        ffn_gain.reshape(1, width),
        routes,
        route_weights,
        branch_gate.reshape(width // SIDE, SIDE),
        cache_keys.reshape(rows, span, HEAD_DIM),
        cache_values.reshape(rows, span, HEAD_DIM),
        query_w,
        key_w,
        value_w,
        out_w,
        exp_gate,
        exp_up,
        exp_down,
        dense_gate,
        dense_up,
        dense_down,
    )
    count = len(results)
    return pl.pallas_call(
        functools.partial(finish_kernel, count),
        name="finish",
        out_shape=tuple(jax.ShapeDtypeStruct(r.shape, r.dtype) for r in results),
        in_specs=[anywhere] * count,
        out_specs=(anywhere,) * count,
        scratch_shapes=[pltpu.VMEM(r.shape, r.dtype) for r in results] + [sem((count,)), sem((count,))],
        compiler_params=pltpu.CompilerParams(vmem_limit_bytes=63 * 2**20),
    )(*results)


def solution(mesh):
    placed = (
        P("ep", None),
        P("ep"),
        P("ep", None, None, None),
        P("ep", None, None, None),
        P(),
        P(),
        P(),
        P(),
        P(),
        P(),
        P(),
        P(),
        P("ep", None),
        P("ep", None),
        P(None, "ep"),
        P(None, "ep"),
        P("ep", None),
        P("ep", None, None),
        P("ep", None, None),
        P("ep", None, None),
        P(),
    )
    return jax.shard_map(
        functools.partial(per_device, mesh.shape["ep"]),
        mesh=mesh,
        in_specs=placed,
        out_specs=(P("ep", None), P("ep", None), P("ep", None)),
        check_vma=False,
    )
```

profile of v0, /device:TPU:0, one launch (start us, length us, event | category | flops | bytes accessed | tf_op | source)
XLA Modules:
  0.0 42.8 jit_solution(6533639519543868903)
XLA Ops:
  0.6 40.7 %layer.1 = (bf16[4,2048]{1,0:T(4,128)(2,1)}, bf16[4,256]{1,0:T(4,128)(2,1)}, bf16[4,256]{1,0:T(4,128)(2,1)}) custom-call(bf16[4,2048]{1,0:T(4,128)(2,1)} %tokens.1, s32[4]{0:T(128)} %lengths.1, f32[8]{0:T(128)} %lam.1, f32[1,128]{1,0:T(1,128)} %bitcast.19, f32[1,2048]{1,0:T(1,128)} %bitcast.14, f32[1,2048]{1,0:T(1,128)} %bitcast.15, s32[2,4]{1,0:T(2,128)} %bitcast.17, ...), custom_call_target="tpu_custom_call" | custom-call | tf_op jit(solution)/shard_map/layer/pallas_call | solution.py:631
  41.4 1.4 %finish.1 = (bf16[4,2048]{1,0:T(4,128)(2,1)}, bf16[4,256]{1,0:T(4,128)(2,1)}, bf16[4,256]{1,0:T(4,128)(2,1)}) custom-call(bf16[4,2048]{1,0:T(4,128)(2,1)} %get-tuple-element.6.refs_0_, bf16[4,256]{1,0:T(4,128)(2,1)} %get-tuple-element.7.refs_1_, bf16[4,256]{1,0:T(4,128)(2,1)} %get-tuple-element.8.refs_2_), custom_call_target="tpu_custom_call" | custom-call | tf_op jit(solution)/shard_map/finish/pallas_call | solution.py:725
where the time goes:
time: 43 us; the launch traced here: 42.8 us
  Pallas kernels  42.1 us (98%)
  between operations  0.65 us (2%)
    pallas_call x1, Pallas kernels, per_device(): pl.pallas_call(functools.partial(layer_kernel, n), name='layer', out_shap...  40.7 us
    pallas_call x1, Pallas kernels, per_device(): pl.pallas_call(functools.partial(finish_kernel, count), name='finish', ou...  1.38 us

commit v1 on v0

--- a/solution.py
+++ b/solution.py
@@ -46,6 +46,7 @@
     vsem,
     osem,
     more_loads,
+    once_entered,
 ):
     tokens, lengths, lam, head_gain, attn_gain, ffn_gain, routes, route_weights, branch_gate = [
         dst for _, dst in small[0]
@@ -58,8 +59,9 @@
     small_copies = [
         pltpu.make_async_copy(src, dst, small[1].at[i]) for i, (src, dst) in enumerate(small[0])
     ]
-    for copy in small_copies:
-        copy.start()
+    early, late = (0, 4), (1, 2, 3, 5, 6, 7, 8)
+    for i in early + late:
+        small_copies[i].start()
     weight_copies = []
     for c in range(QKV_CHUNKS):
         part = pl.ds(c * step, step)
@@ -77,10 +79,9 @@
         value_copies[s].start()
     out_copy = pltpu.make_async_copy(out_w, obuf, osem.at[0])
     out_copy.start()
-    for copy in more_loads:
-        copy.start()
-    for copy in small_copies:
-        copy.wait()
+    for i in early:
+        small_copies[i].wait()
+    once_entered()
 
     x = tokens[...].astype(F32)
     normed = x * lax.rsqrt(jnp.mean(x * x, axis=-1, keepdims=True) + 1e-06) * attn_gain[...]
@@ -96,6 +97,8 @@
         query += jnp.dot(left, qbuf[part, :], preferred_element_type=F32)
         knew += jnp.dot(left, kwbuf[part, :], preferred_element_type=F32)
         vnew += jnp.dot(left, vwbuf[part, :], preferred_element_type=F32)
+    for copy in more_loads:
+        copy.start()
     new_keys[...] = knew.astype(BF16)
     new_values[...] = vnew.astype(BF16)
     query = query.astype(BF16).astype(F32)
@@ -105,6 +108,8 @@
         for h in range(HEADS):
             qscr[s, h : h + 1, :] = query[s : s + 1, h * HEAD_DIM : (h + 1) * HEAD_DIM]
 
+    for i in late[:3]:
+        small_copies[i].wait()
     scale = half ** (-0.5)
     lane = lax.broadcasted_iota(jnp.int32, (HEADS, HEAD_DIM), 1)
     head_row = lax.broadcasted_iota(jnp.int32, (HEADS, HEAD_DIM), 0)
@@ -147,6 +152,8 @@
         normal = normal * head_gain[...]
         for h in range(HEADS):
             hscr[s : s + 1, h * HEAD_DIM : (h + 1) * HEAD_DIM] = normal[h : h + 1, :]
+    for i in late[3:]:
+        small_copies[i].wait()
     out_copy.wait()
     state = x + jnp.dot(hscr[...].astype(BF16), obuf[...], preferred_element_type=F32)
     hidden[...] = state
@@ -169,6 +176,11 @@
             table = table + jnp.where(here, route_weights[k, s], 0.0)
     high = table.astype(BF16).astype(F32)
     ext[:, width:] = jnp.where(spot < SIDE // 2, high, table - high).astype(BF16)
+
+
+def shared_cols(cols, blocks):
+    share = cols % 128 if blocks == 2 else 0
+    return share if 2 * share <= cols and share % 16 == 0 else 0
 
 
 def layer_kernel(
@@ -227,20 +239,21 @@
     dgbuf,
     dubuf,
     ddbuf,
+    dswap,
     recv,
     xall,
     gpart,
     upart,
-    gsend,
-    usend,
-    grecv,
-    urecv,
+    gusend,
+    gurecv,
     act,
     total,
     sib_send,
     sib_recv,
     rs_send,
     rs_recv,
+    far_send,
+    far_recv,
     wsem,
     ag_send_sem,
     ag_recv_sem,
@@ -252,6 +265,9 @@
     sib_recv_sem,
     rs_send_sem,
     rs_recv_sem,
+    far_send_sem,
+    far_recv_sem,
+    swap_sem,
 ):
     me = lax.axis_index("ep")
     chips = n // 2
@@ -286,19 +302,39 @@
         home = lax.rem(block + blocks - b, blocks)
         return home * SPLIT + lax.rem(gchip + gchips - j, gchips) * 2 + core
 
-    loads = [
-        pltpu.make_async_copy(src, dst, wsem.at[i])
-        for i, (src, dst) in enumerate(
-            (
-                (dense_gate.at[0], dgbuf),
-                (dense_up.at[0], dubuf),
-                (exp_gate, egbuf),
-                (exp_up, eubuf),
-                (exp_down, edbuf),
-                (dense_down.at[0], ddbuf),
-            )
+    hidden_cols = dense_gate.shape[1]
+    share = shared_cols(hidden_cols, blocks)
+    rest = hidden_cols - 2 * share
+    keep = share + rest
+    pitch = gusend.shape[1] // 2
+    if share:
+        mine = pl.multiple_of(block * share, 16)
+        theirs = pl.multiple_of((1 - block) * share, 16)
+        in_pieces = [(theirs, 0, share), (2 * share, share, rest), (mine, keep, share), (2 * share, keep + share, rest)]
+        out_pieces = [(mine, 0, share), (2 * share, share, rest)]
+    else:
+        in_pieces = out_pieces = [(0, 0, hidden_cols)]
+
+    def pieces_of(src, dst, pieces):
+        return [(src.at[0, pl.ds(a, size)], dst.at[pl.ds(b, size)]) for a, b, size in pieces]
+
+    pairs = [
+        pieces_of(dense_gate, dgbuf, in_pieces) + pieces_of(dense_up, dubuf, in_pieces),
+        [(exp_gate, egbuf), (exp_up, eubuf)],
+        [(exp_down, edbuf)],
+        pieces_of(dense_down, ddbuf, out_pieces),
+    ]
+    load_sets = []
+    for pair_set in pairs:
+        first = sum(len(x) for x in load_sets)
+        load_sets.append(
+            [pltpu.make_async_copy(src, dst, wsem.at[first + i]) for i, (src, dst) in enumerate(pair_set)]
         )
-    ]
+
+    def wait_loads(k):
+        for copy in load_sets[k]:
+            copy.wait()
+
     barrier = pltpu.get_barrier_semaphore()
 
     def greet(k, carry):
@@ -307,6 +343,25 @@
 
     lax.fori_loop(1, chips, greet, 0)
     pl.semaphore_signal(barrier, inc=1, device_id=(sibling,), device_id_type=MESH)
+
+    swaps = []
+    if share:
+        swaps = [
+            pltpu.make_async_remote_copy(
+                src_ref=dense_down.at[0, pl.ds(theirs, share)],
+                dst_ref=dswap,
+                send_sem=swap_sem.at[0],
+                recv_sem=swap_sem.at[1],
+                device_id=(lax.rem(me + SPLIT, n),),
+                device_id_type=MESH,
+            )
+        ]
+
+    def once_entered():
+        pl.semaphore_wait(barrier, chips)
+        for copy in swaps:
+            copy.start()
+
     small = [
         (tokens, tokens_v),
         (lengths, lengths_v),
@@ -321,9 +376,8 @@
     attention_part(
         experts, (small, small_sem), keys, values, query_w, key_w, value_w, out_w, ext, hidden,
         new_keys, new_values, kbuf, vbuf, qbuf, kwbuf, vwbuf, obuf, qscr, hscr,
-        asem, ksem, vsem, osem, loads,
+        asem, ksem, vsem, osem, sum(load_sets, []), once_entered,
     )
-    pl.semaphore_wait(barrier, chips)
 
     def send_block(ref, owner, q, target):
         return pltpu.make_async_remote_copy(
@@ -412,39 +466,44 @@
 
             lax.fori_loop(0, total_rows // chunk, run, 0)
 
-    loads[0].wait()
-    loads[1].wait()
+    wait_loads(0)
 
     def dense_in(part):
         left = xall[part, pl.ds(pl.multiple_of(block * row_span, 128), row_span)].astype(BF16)
         across = (((1,), (1,)), ((), ()))
-        g = lax.dot_general(left, dgbuf[...], across, preferred_element_type=F32)
-        u = lax.dot_general(left, dubuf[...], across, preferred_element_type=F32)
+
+        def product(buf, at):
+            return lax.dot_general(left, buf[at : at + keep, :], across, preferred_element_type=F32)
+
+        g, u = product(dgbuf, 0), product(dubuf, 0)
+        gusend[part, :keep] = g.astype(BF16)
+        gusend[part, pitch : pitch + keep] = u.astype(BF16)
+        if share:
+            g, u = product(dgbuf, keep), product(dubuf, keep)
         gpart[part, :] = g
         upart[part, :] = u
-        gsend[part, :] = g.astype(BF16)
-        usend[part, :] = u.astype(BF16)
 
     def exchange(b):
         part = group_part(b)
         copies = []
         for j in range(1, blocks):
-            for i, (src, dst) in enumerate(((gsend, grecv), (usend, urecv))):
-                slot = 2 * (b * (blocks - 1) + j - 1) + i
-                copies.append(
-                    pltpu.make_async_remote_copy(
-                        src_ref=src.at[part],
-                        dst_ref=dst.at[j - 1, part],
-                        send_sem=ex_send_sem.at[slot],
-                        recv_sem=ex_recv_sem.at[slot],
-                        device_id=(lax.rem(me + j * SPLIT, n),),
-                        device_id_type=MESH,
-                    )
+            slot = b * (blocks - 1) + j - 1
+            copies.append(
+                pltpu.make_async_remote_copy(
+                    src_ref=gusend.at[part],
+                    dst_ref=gurecv.at[j - 1, part],
+                    send_sem=ex_send_sem.at[slot],
+                    recv_sem=ex_recv_sem.at[slot],
+                    device_id=(lax.rem(me + j * SPLIT, n),),
+                    device_id_type=MESH,
                 )
+            )
         for copy in copies:
             copy.start()
         return copies
 
+    if keep < pitch:
+        gusend[...] = jnp.zeros_like(gusend)
     widen(block)
     dense_in(group_part(0))
     exchanges = [exchange(0)]
@@ -462,8 +521,7 @@
         dense_in(group_part(b))
         exchanges.append(exchange(b))
 
-    loads[2].wait()
-    loads[3].wait()
+    wait_loads(1)
 
     def expert_in(part):
         left = xall[part, :width].astype(BF16)
@@ -472,7 +530,7 @@
         act[part, :] = (g / (1.0 + jnp.exp(-g)) * u).astype(BF16)
 
     by_rows(expert_in)
-    loads[4].wait()
+    wait_loads(2)
 
     def side_value(part, which):
         side = xall[part, width:]
@@ -484,18 +542,25 @@
         total[part, :] = product * side_value(part, expert)
 
     by_rows(expert_out)
-    loads[5].wait()
+    wait_loads(3)
+    for copy in swaps:
+        copy.wait_recv()
 
     def dense_out(part):
         g = gpart[part, :]
         u = upart[part, :]
         for j in range(blocks - 1):
-            g = g + grecv[j, part, :].astype(F32)
-            u = u + urecv[j, part, :].astype(F32)
+            g = g + gurecv[j, part, :keep].astype(F32)
+            u = u + gurecv[j, part, pitch : pitch + keep].astype(F32)
         dact = (g / (1.0 + jnp.exp(-g)) * u).astype(BF16)
         product = jnp.dot(dact, ddbuf[...], preferred_element_type=F32)
         cols = pl.ds(pl.multiple_of(block * row_span, 128), row_span)
-        total[part, cols] = total[part, cols] + product * side_value(part, experts)
+        gate = side_value(part, experts)
+        total[part, cols] = total[part, cols] + product * gate
+        if share:
+            across = jnp.dot(dact[:, :share], dswap[...], preferred_element_type=F32)
+            cols = pl.ds(pl.multiple_of((1 - block) * row_span, 128), row_span)
+            total[part, cols] = total[part, cols] + across * gate
 
     def both_halves(d, j):
         c = place(d, j)
@@ -519,9 +584,26 @@
             dst_ref=rs_recv.at[q],
             send_sem=rs_send_sem.at[q],
             recv_sem=rs_recv_sem.at[q],
-            device_id=(place(d, j) * 2 + core,),
+            device_id=(mate(j),),
             device_id_type=MESH,
         )
+
+    def cross_copy(d):
+        return pltpu.make_async_remote_copy(
+            src_ref=far_send.at[d - 1],
+            dst_ref=far_recv.at[d - 1],
+            send_sem=far_send_sem.at[d - 1],
+            recv_sem=far_recv_sem.at[d - 1],
+            device_id=(group(d) * SPLIT + lax.rem(me, SPLIT),),
+            device_id_type=MESH,
+        )
+
+    def collect(d, acc):
+        def one(j, acc):
+            rs_copy(d, j).wait_recv()
+            return acc + rs_recv[d * gchips + j].astype(F32)
+
+        return lax.fori_loop(1, gchips, one, acc)
 
     def add_sibling(d, j):
         q = d * gchips + j
@@ -531,9 +613,7 @@
 
     for d in list(range(1, blocks)) + [0]:
         for j in range(1, blocks):
-            first = 2 * (j - 1)
-            for copy in exchanges[(j + d) % blocks][first : first + 2]:
-                copy.wait_recv()
+            exchanges[(j + d) % blocks][j - 1].wait_recv()
         dense_out(group_part(d))
 
         def pack(j):
@@ -546,21 +626,23 @@
 
         loop(0, gchips, pack)
         loop(0, gchips, lambda j: sib_copy(d * gchips + j).start())
-        loop(1 if d == 0 else 0, gchips, forward)
-    result = hidden[...] + add_sibling(0, 0)
-
-    def collect(q, acc):
-        rs_copy(q // gchips, lax.rem(q, gchips)).wait_recv()
-        return acc + rs_recv[q].astype(F32)
-
-    result = lax.fori_loop(1, chips, collect, result)
+        loop(1, gchips, forward)
+    for far in range(1, blocks):
+        reduced = collect(far, add_sibling(far, 0))
+        far_send[far - 1] = reduced.astype(BF16)
+        cross_copy(far).start()
+    result = collect(0, hidden[...] + add_sibling(0, 0))
+    for d in range(1, blocks):
+        cross_copy(d).wait_recv()
+        result = result + far_recv[d - 1].astype(F32)
     out[...] = result.astype(BF16)
 
     for b in range(1, blocks):
         far_copy(b).wait_send()
         loop(1, gchips, lambda j: relay_copy(b, j).wait_send())
         loop(0, gchips, lambda j: fw_copy(b, j).wait_send())
-        loop(0, gchips, lambda j: rs_copy(b, j).wait_send())
+        loop(1, gchips, lambda j: rs_copy(b, j).wait_send())
+        cross_copy(b).wait_send()
     own_copy.wait_send()
 
     def drain(j):
@@ -570,22 +652,17 @@
 
     loop(1, gchips, drain)
     loop(0, chips, lambda q: sib_copy(q).wait_send())
-    for copies in exchanges:
+    for copies in exchanges + [swaps]:
         for copy in copies:
             copy.wait_send()
 
 
 def finish_kernel(count, *refs):
-    sources, targets, held = refs[:count], refs[count : 2 * count], refs[2 * count : 3 * count]
-    in_sem, out_sem = refs[3 * count :]
-    ins = [pltpu.make_async_copy(sources[i], held[i], in_sem.at[i]) for i in range(count)]
-    outs = [pltpu.make_async_copy(held[i], targets[i], out_sem.at[i]) for i in range(count)]
-    for copy in ins:
+    sources, targets, sem = refs[:count], refs[count : 2 * count], refs[2 * count]
+    copies = [pltpu.make_async_copy(sources[i], targets[i], sem.at[i]) for i in range(count)]
+    for copy in copies:
         copy.start()
-    for i in range(count):
-        ins[i].wait()
-        outs[i].start()
-    for copy in outs:
+    for copy in copies:
         copy.wait()
 
 
@@ -622,6 +699,10 @@
     all_rows = n * rows
     chips = n // 2
     cols = dense_gate.shape[2]
+    share = shared_cols(cols, n // SPLIT)
+    keep = cols - share
+    pitch = -(-keep // 128) * 128
+    in_rows = 2 * keep if share else cols
     others = max(1, n // SPLIT - 1)
     sem = pltpu.SemaphoreType.DMA
     dense_gate = jnp.swapaxes(dense_gate, 1, 2)
@@ -632,9 +713,9 @@
         functools.partial(layer_kernel, n),
         name="layer",
         out_shape=(
-            jax.ShapeDtypeStruct((rows, width), BF16),
-            jax.ShapeDtypeStruct((rows, key_w.shape[1]), BF16),
-            jax.ShapeDtypeStruct((rows, value_w.shape[1]), BF16),
+            pltpu.VMEM((rows, width), BF16),
+            pltpu.VMEM((rows, key_w.shape[1]), BF16),
+            pltpu.VMEM((rows, value_w.shape[1]), BF16),
         ),
         in_specs=[anywhere] * 21,
         out_specs=(vmem,) * 3,
@@ -666,34 +747,38 @@
             pltpu.VMEM(exp_gate.shape, BF16),
             pltpu.VMEM(exp_up.shape, BF16),
             pltpu.VMEM(exp_down.shape, BF16),
-            pltpu.VMEM(dense_gate.shape[1:], BF16),
-            pltpu.VMEM(dense_up.shape[1:], BF16),
-            pltpu.VMEM(dense_down.shape[1:], BF16),
+            pltpu.VMEM((in_rows, dense_gate.shape[2]), BF16),
+            pltpu.VMEM((in_rows, dense_up.shape[2]), BF16),
+            pltpu.VMEM((keep, dense_down.shape[2]), BF16),
+            pltpu.VMEM((max(share, 16), dense_down.shape[2]), BF16),
             pltpu.VMEM((n, rows, width + SIDE), BF16),
             pltpu.VMEM((all_rows, width + SIDE), F32),
-            pltpu.VMEM((all_rows, cols), F32),
-            pltpu.VMEM((all_rows, cols), F32),
-            pltpu.VMEM((all_rows, cols), BF16),
-            pltpu.VMEM((all_rows, cols), BF16),
-            pltpu.VMEM((others, all_rows, cols), BF16),
-            pltpu.VMEM((others, all_rows, cols), BF16),
+            pltpu.VMEM((all_rows, keep), F32),
+            pltpu.VMEM((all_rows, keep), F32),
+            pltpu.VMEM((all_rows, 2 * pitch), BF16),
+            pltpu.VMEM((others, all_rows, 2 * pitch), BF16),
             pltpu.VMEM((all_rows, exp_gate.shape[1]), BF16),
             pltpu.VMEM((all_rows, width), F32),
             pltpu.VMEM((chips, rows, width), BF16),
             pltpu.VMEM((chips, rows, width), BF16),
             pltpu.VMEM((chips, rows, width), BF16),
             pltpu.VMEM((chips, rows, width), BF16),
-            sem((6,)),
+            pltpu.VMEM((others, rows, width), BF16),
+            pltpu.VMEM((others, rows, width), BF16),
+            sem((13,)),
             sem((chips,)),
             sem((chips,)),
             sem((chips,)),
             sem((chips,)),
-            sem((2 * others * (n // SPLIT),)),
-            sem((2 * others * (n // SPLIT),)),
+            sem((others * (n // SPLIT),)),
+            sem((others * (n // SPLIT),)),
             sem((chips,)),
             sem((chips,)),
             sem((chips,)),
             sem((chips,)),
+            sem((others,)),
+            sem((others,)),
+            sem((2,)),
         ],
         compiler_params=pltpu.CompilerParams(
             collective_id=0, has_side_effects=True, vmem_limit_bytes=63 * 2**20
@@ -726,10 +811,10 @@
         functools.partial(finish_kernel, count),
         name="finish",
         out_shape=tuple(jax.ShapeDtypeStruct(r.shape, r.dtype) for r in results),
-        in_specs=[anywhere] * count,
+        in_specs=[vmem] * count,
         out_specs=(anywhere,) * count,
-        scratch_shapes=[pltpu.VMEM(r.shape, r.dtype) for r in results] + [sem((count,)), sem((count,))],
-        compiler_params=pltpu.CompilerParams(vmem_limit_bytes=63 * 2**20),
+        scratch_shapes=[sem((count,))],
+        compiler_params=pltpu.CompilerParams(vmem_limit_bytes=2**20),
     )(*results)
 
 

time: 43 us -> 36.6 us (0.85)
  Pallas kernels: 42.1 us -> 35.8 us
    pallas_call x1, Pallas kernels: 40.7 us -> 35.2 us  [per_device(): pl.pallas_call(functools.partial(layer_kernel, n), name='layer', out_shap...]
    pallas_call x1, Pallas kernels: 1.38 us -> 0.64 us  [per_device(): pl.pallas_call(functools.partial(finish_kernel, count), name='finish', ou...]
where the time goes in v1:
time: 36.6 us; the launch traced here: 36.5 us
  Pallas kernels  35.8 us (98%)
  between operations  0.65 us (2%)
    pallas_call x1, Pallas kernels, per_device(): pl.pallas_call(functools.partial(layer_kernel, n), name='layer', out_shap...  35.2 us

profile of v1, /device:TPU:0, one launch (start us, length us, event | category | flops | bytes accessed | tf_op | source)
XLA Modules:
  0.0 36.5 jit_solution(15404664623235431950)
XLA Ops:
  0.6 35.2 %layer.1 = (bf16[4,2048]{1,0:T(4,128)(2,1)S(1)}, bf16[4,256]{1,0:T(4,128)(2,1)S(1)}, bf16[4,256]{1,0:T(4,128)(2,1)S(1)}) custom-call(bf16[4,2048]{1,0:T(4,128)(2,1)} %tokens.1, s32[4]{0:T(128)} %lengths.1, f32[8]{0:T(128)} %lam.1, f32[1,128]{1,0:T(1,128)} %bitcast.19, f32[1,2048]{1,0:T(1,128)} %bitcast.14, f32[1,2048]{1,0:T(1,128)} %bitcast.15, ...), custom_call_target="tpu_custom_call" | custom-call | tf_op jit(solution)/shard_map/layer/pallas_call | solution.py:712
  35.8 0.6 %finish.1 = (bf16[4,2048]{1,0:T(4,128)(2,1)}, bf16[4,256]{1,0:T(4,128)(2,1)}, bf16[4,256]{1,0:T(4,128)(2,1)}) custom-call(bf16[4,2048]{1,0:T(4,128)(2,1)S(1)} %get-tuple-element.6.refs_0_, bf16[4,256]{1,0:T(4,128)(2,1)S(1)} %get-tuple-element.7.refs_1_, bf16[4,256]{1,0:T(4,128)(2,1)S(1)} %get-tuple-element.8.refs_2_), custom_call_target="tpu_custom_call" | custom-call | tf_op jit(solution)/shard_map/finish/pallas_call | solution.py:810
